TPU v7x, 512 devices: a 4x2x32 block of a 4x8x32 slice. The times are simulated.
512 devices in a mesh: grp: 2 (over y), sp: 64 (over z, core), tp: 4 (over x).
Axes of the slice: x: 4, y: 2, z: 32, core: 2. Of those that a mesh axis runs over, the one named last changes fastest.
The devices are a block of a 4x8x32 slice.
Arguments:
- recurrent_query: bfloat16 [32768, 1024], P(('grp', 'sp'), 'tp'), parts along dimension 0, may hold values from -6 to 6
- recurrent_forget_gate: bfloat16 [32768, 1024], P(('grp', 'sp'), 'tp'), parts along dimension 0, may hold values from -4.5 to 4.5
- recurrent_value: bfloat16 [32768, 1024], P(('grp', 'sp'), 'tp'), parts along dimension 0, may hold values from -6 to 6
- recurrent_gate_lower_bound: float32 [1024], P('tp'), may hold values from 1.5 to 14
- recurrent_added_decay: float32 [32768, 8], P(('grp', 'sp'), 'tp'), parts along dimension 0, may hold values from -0.51 to 0
- recurrent_norm_gain: float32 [128], replicated, may hold values from 0.1 to 1.9
- attention_query_first: bfloat16 [32768, 512], P(('grp', 'sp'), 'tp'), parts along dimension 0, may hold values from -20 to 20
- attention_key_first: bfloat16 [32768, 256], P(('grp', 'sp'), 'tp'), parts along dimension 0, may hold values from -20 to 20
- attention_query_second: bfloat16 [32768, 512], P(('grp', 'sp'), 'tp'), parts along dimension 0, may hold values from -20 to 20
- attention_key_second: bfloat16 [32768, 256], P(('grp', 'sp'), 'tp'), parts along dimension 0, may hold values from -20 to 20
- attention_value: bfloat16 [32768, 512], P(('grp', 'sp'), 'tp'), parts along dimension 0, may hold values from -6 to 6
- second_map_weight: float32 [8], P('tp'), may hold values from 0.3 to 0.8
- attention_norm_gain: float32 [128], replicated, may hold values from 0.1 to 1.9
- output_weight: bfloat16 [2, 1024, 2048], P(None, 'tp', 'sp'), may hold values from -0.125 to 0.125
Outputs:
- mixed: bfloat16 [32768, 2048], P(('grp', 'sp', 'tp')), parts along dimension 0
There are 2 independent parts, one for each index of `grp`. A program takes and returns all parts, laid end to end along the dimension named above; an argument that names none is the same for every part. Nothing has to cross between parts.
All inputs are finite; a program needn't handle non-finite values.
Results may differ from a plain program's by a relative error of at most 0.02.
Values may be sent and summed in bfloat16 or wider, within the bound.
A program may use at most 64 MiB of HBM per device.

v0:
```python
import jax
import jax.numpy as jnp
from jax import lax
from jax.sharding import PartitionSpec as P

HG_DK = 128
HG_DV = 128
DA_HD = 64
BLK = 32
epsilon = 1e-06
key_span = 512


def carried_in(array, axis, combine, identity):
    size, place = (lax.axis_size(axis), lax.axis_index(axis))
    everything = jax.tree.map(
        lambda part, kind: lax.all_gather(part.astype(kind), axis),
        array,
        (jnp.bfloat16, jnp.bfloat16),
    )
    start = jax.tree.map(
        lambda part, zero: jnp.broadcast_to(jnp.asarray(zero, part.dtype), part.shape),
        array,
        identity,
    )

    def hop(k, before):
        reached = k < place
        new = combine(
            before, jax.tree.map(lambda part, own: part[k].astype(own.dtype), everything, array)
        )
        return jax.tree.map(lambda a, b: jnp.where(reached, a, b), new, before)

    return lax.fori_loop(0, size, hop, start)


def in_one_piece(arrays, axis, dim, along):
    ends, at = ([], 0)
    for a in arrays[:-1]:
        at += a.shape[along]
        ends.append(at)
    both = jnp.concatenate(arrays, axis=along)
    return tuple(jnp.split(lax.all_gather(both, axis, axis=dim, tiled=True), ends, axis=along))


def split_up(array, dim, size):
    before, after = (array.shape[:dim], array.shape[dim + 1 :])
    return jnp.moveaxis(array.reshape(*before, size, -1, *after), dim, 0)


def summed_on_arrival(array, axis, dim):
    size = lax.axis_size(axis)
    pieces = lax.all_to_all(split_up(array, dim, size), axis, 0, 0, tiled=True)
    return jnp.sum(pieces.astype(jnp.float32), axis=0)


def head_norm(head_values, gain_vec):
    mean_square = jnp.mean(head_values * head_values, axis=-1, keepdims=True)
    return head_values * lax.rsqrt(mean_square + epsilon) * gain_vec


def decay_factors(gate_preactivation, lower_bound_logit, added_log_decay, number_of_heads):
    token_count = gate_preactivation.shape[0]
    floor_rate = jax.nn.sigmoid(-lower_bound_logit).reshape(number_of_heads, -1)
    state_inflow = floor_rate[None] * jax.nn.sigmoid(
        -gate_preactivation.astype(jnp.float32)
    ).reshape(token_count, number_of_heads, -1)
    decay_logarithm = jnp.log1p(-state_inflow) + added_log_decay[:, :, None]
    return (state_inflow, decay_logarithm)


def recurrence_blocks(queries, decay_logarithm, state_inflow, value_rows, block_len):
    token_count, number_of_heads, key_width = queries.shape
    block_count = token_count // block_len

    def to_blocks(source):
        return source.reshape(block_count, block_len, number_of_heads, source.shape[-1])

    causal = jnp.tril(jnp.ones((block_len, block_len), jnp.float32))[:, :, None, None]

    def block_step(carry_state, inputs):
        query_blk, decay_blk, inflow_blk, value_blk = inputs
        cumulative = jnp.cumsum(decay_blk, axis=0)
        relative = cumulative[:, None] - cumulative[None, :]
        decay_table = jnp.exp(jnp.minimum(relative, 0.0)) * causal
        scores = jnp.einsum("thd,shd,tshd->hts", query_blk, inflow_blk, decay_table)
        block_out = jnp.einsum("hts,shv->thv", scores, value_blk)
        block_out = block_out + jnp.einsum(
            "thd,hdv->thv", query_blk * jnp.exp(cumulative), carry_state
        )
        last_log = cumulative[-1]
        new_state = jnp.exp(last_log)[:, :, None] * carry_state + jnp.einsum(
            "shd,shv->hdv", inflow_blk * jnp.exp(last_log[None] - cumulative), value_blk
        )
        return (new_state, block_out)

    zero_state = jnp.zeros((number_of_heads, key_width, value_rows.shape[-1]), jnp.float32)
    final_state, outputs = lax.scan(
        block_step,
        zero_state,
        (
            to_blocks(queries),
            to_blocks(decay_logarithm),
            to_blocks(state_inflow),
            to_blocks(value_rows),
        ),
    )
    return (final_state, outputs.reshape(token_count, number_of_heads, -1))


def chain_pair(earlier, following):
    return (earlier[0] * following[0], following[0][:, :, None] * earlier[1] + following[1])


def recurrent_path_output(
    recurrent_query,
    recurrent_forget_gate,
    recurrent_value,
    recurrent_gate_lower_bound,
    recurrent_added_decay,
    recurrent_norm_gain,
):
    token_count = recurrent_query.shape[0]
    number_of_heads = recurrent_gate_lower_bound.shape[0] // HG_DK
    state_inflow, decay_logarithm = decay_factors(
        recurrent_forget_gate, recurrent_gate_lower_bound, recurrent_added_decay, number_of_heads
    )
    queries = recurrent_query.astype(jnp.float32).reshape(token_count, number_of_heads, HG_DK)
    value_rows = recurrent_value.astype(jnp.float32).reshape(token_count, number_of_heads, HG_DV)
    final_state, local_out = recurrence_blocks(
        queries, decay_logarithm, state_inflow, value_rows, BLK
    )
    running_log = jnp.cumsum(decay_logarithm, axis=0)
    through = jnp.exp(running_log[-1])
    incoming = carried_in(
        (through, final_state),
        "sp",
        chain_pair,
        (jnp.ones_like(through), jnp.zeros_like(final_state)),
    )
    carried = jnp.einsum("thd,hdv->thv", queries * jnp.exp(running_log), incoming[1])
    return (
        head_norm(local_out + carried, recurrent_norm_gain)
        .astype(jnp.bfloat16)
        .reshape(token_count, -1)
    )


def attention_branch(
    attention_query_first,
    attention_key_first,
    attention_query_second,
    attention_key_second,
    attention_value,
    second_map_weight,
    attention_norm_gain,
):
    query_rows = attention_query_first.shape[0]
    key_heads = attention_key_first.shape[1] // DA_HD
    group_size = attention_query_first.shape[1] // DA_HD // key_heads
    score_scale = DA_HD ** (-0.5)
    offset = lax.axis_index("sp") * query_rows
    query_pos = offset + jnp.arange(query_rows)
    last_query = offset + query_rows - 1
    queries_one = attention_query_first.reshape(query_rows, key_heads, group_size, DA_HD)
    queries_two = attention_query_second.reshape(query_rows, key_heads, group_size, DA_HD)

    def map_update(running, queries, key_rows, value_rows, allowed):
        row_max, weight_mass, value_sum = running
        scores = (
            jnp.einsum("qkgd,skd->kgqs", queries, key_rows, preferred_element_type=jnp.float32)
            * score_scale
        )
        scores = jnp.where(allowed, scores, -1e30)
        new_max = jnp.maximum(row_max, jnp.max(scores, axis=-1))
        weights = jnp.where(allowed, jnp.exp(scores - new_max[..., None]), 0.0)
        shrink = jnp.exp(row_max - new_max)
        weight_mass = weight_mass * shrink + jnp.sum(weights, axis=-1)
        value_sum = value_sum * shrink[..., None] + jnp.einsum(
            "plew,wpd->pled",
            weights.astype(jnp.bfloat16),
            value_rows,
            preferred_element_type=jnp.float32,
        )
        return (new_max, weight_mass, value_sum)

    def key_block(running, block_one, block_two, block_values, first_row):
        span_rows = block_one.shape[0]
        key_pos = first_row + jnp.arange(span_rows)
        allowed = key_pos[None, :] <= query_pos[:, None]
        shaped_one = block_one.reshape(span_rows, key_heads, DA_HD)
        shaped_two = block_two.reshape(span_rows, key_heads, DA_HD)
        shaped_values = block_values.reshape(span_rows, key_heads, 2 * DA_HD)
        return (
            map_update(running[0], queries_one, shaped_one, shaped_values, allowed),
            map_update(running[1], queries_two, shaped_two, shaped_values, allowed),
        )

    def guarded_block(running, block_one, block_two, block_values, first_row):

        def compute(state_in):
            return key_block(state_in, block_one, block_two, block_values, first_row)

        def unchanged(state_in):
            return state_in

        result = lax.cond(first_row > last_query, unchanged, compute, running)
        return result

    start_max = jnp.full((key_heads, group_size, query_rows), -1e30, jnp.float32)
    zero_mass = jnp.zeros((key_heads, group_size, query_rows), jnp.float32)
    zero_sum = jnp.zeros((key_heads, group_size, query_rows, 2 * DA_HD), jnp.float32)
    fresh_state = (start_max, zero_mass, zero_sum)
    running = (fresh_state, fresh_state)
    shard_one, shard_two, shard_values = in_one_piece(
        (attention_key_first, attention_key_second, attention_value), "sp", 0, 1
    )
    row_count = shard_one.shape[0]
    span_rows = min(row_count, key_span)
    full_count = row_count // span_rows

    def span_step(span_index, state_in):
        begin_row = span_index * span_rows
        return guarded_block(
            state_in,
            lax.dynamic_slice_in_dim(shard_one, begin_row, span_rows, 0),
            lax.dynamic_slice_in_dim(shard_two, begin_row, span_rows, 0),
            lax.dynamic_slice_in_dim(shard_values, begin_row, span_rows, 0),
            begin_row,
        )

    running = lax.fori_loop(0, full_count, span_step, running)
    first_map, second_map = running
    lambda_table = second_map_weight.reshape(key_heads, group_size)[:, :, None, None]
    combined = first_map[2] / first_map[1][..., None] - lambda_table * (
        second_map[2] / second_map[1][..., None]
    )
    combined = jnp.transpose(combined, (2, 0, 1, 3)).reshape(
        query_rows, key_heads * group_size, 2 * DA_HD
    )
    return head_norm(combined, attention_norm_gain).astype(jnp.bfloat16).reshape(query_rows, -1)


def shards(
    recurrent_query,
    recurrent_forget_gate,
    recurrent_value,
    recurrent_gate_lower_bound,
    recurrent_added_decay,
    recurrent_norm_gain,
    attention_query_first,
    attention_key_first,
    attention_query_second,
    attention_key_second,
    attention_value,
    second_map_weight,
    attention_norm_gain,
    output_weight,
):
    attended = attention_branch(
        attention_query_first,
        attention_key_first,
        attention_query_second,
        attention_key_second,
        attention_value,
        second_map_weight,
        attention_norm_gain,
    )
    recurrent_output = recurrent_path_output(
        recurrent_query,
        recurrent_forget_gate,
        recurrent_value,
        recurrent_gate_lower_bound,
        recurrent_added_decay,
        recurrent_norm_gain,
    )
    pieces = lax.all_gather(output_weight, "sp", axis=2, tiled=True)
    partial_terms = jnp.dot(
        recurrent_output, pieces[0], preferred_element_type=jnp.float32
    ) + jnp.dot(attended, pieces[1], preferred_element_type=jnp.float32)
    return summed_on_arrival(partial_terms.astype(jnp.bfloat16), "tp", 0).astype(jnp.bfloat16)


def solution(mesh):
    return jax.shard_map(
        shards,
        mesh=mesh,
        in_specs=(
            P(("grp", "sp"), "tp"),
            P(("grp", "sp"), "tp"),
            P(("grp", "sp"), "tp"),
            P("tp"),
            P(("grp", "sp"), "tp"),
            P(),
            P(("grp", "sp"), "tp"),
            P(("grp", "sp"), "tp"),
            P(("grp", "sp"), "tp"),
            P(("grp", "sp"), "tp"),
            P(("grp", "sp"), "tp"),
            P("tp"),
            P(),
            P(None, "tp", "sp"),
        ),
        out_specs=P(("grp", "sp", "tp"), None),
        check_vma=False,
    )
```

profile of v0, /device:TPU:2016, one launch (start us, length us, event | category | flops | bytes accessed | tf_op | source)
XLA Modules:
  0.0 664.5 jit_solution(9917278042523082611)
XLA Ops:
  11.3 21.9 %while.52 = (s32[]{:T(128)}, f32[2,128,128]{2,1,0:T(8,128)S(1)}, f32[8,32,2,128]{3,1,0,2:T(8,128)S(1)}, f32[8,32,2,128]{3,2,1,0:T(2,128)S(1)}, f32[8,32,2,128]{3...) while((s32[]{:T(128)}, f32[2,128,128]{2,1,0:T(8,128)S(1)}, ...), condition=%wide.region_2.3_spmd.clone, body=%wide.region_0.2_spmd.clone.sunk | while | flops 6725635 | bytes 3266684 | solution.py:98
  36.9 51.6 %all_gather.16 = bf16[64,2,128]{2,1,0:T(2,128)(2,1)S(1)} all-gather(bf16[1,2,128]{2,1,0:T(2,128)(2,1)S(1)} %fusion.67), channel_id=1, replica_groups=mesh['grp'=2,'sp'=64,'tp'=4] {'sp'}, dimensions={0}, use_global_device_ids=true | all-gather | bytes 33280 | tf_op jit(solution)/shard_map/all_gather | solution.py:17
  89.2 64.9 %all-gather.9.cloned.1.call-done = bf16[128,128,128]{2,1,0:T(8,128)(2,1)} async-done(((bf16[2,128,128]{2,1,0:T(8,128)(2,1)}), bf16[128,128,128]{2,1,0:T(8,128)(2,1)}) %all-gather.9.cloned.1.call-update) | async-done | bytes 4194320 | tf_op jit(solution)/shard_map/all_gather | solution.py:17
  154.1 64.9 %while.53 = (s32[]{:T(128)}, f32[2,128,128]{2,1,0:T(8,128)S(1)}, s32[]{:T(128)}, bf16[64,2,128]{2,1,0:T(2,128)(2,1)S(1)}, bf16[64,2,128,128]{3,2,1,0:T(8,128)(2,1)}, /*index=5*/s32[]{:T(128)}, s32[]{:T(128)}) while((s32[]{:T(128)}, f32[2,128,128]{2,1,0:T(8,128)S(1)}, s32[]{:T(128)}, bf16[64,2,128]{2,1,0:T(2,128)(2,1)S(1)}, ...), condition=%wide.region_6.0_spmd.clone, body=%wide.region_5.6_spmd.clone.sunk | while | flops 164100 | bytes 330345 | solution.py:34
  219.4 63.2 %all-gather.5.cloned.1.call-done = bf16[2,256,2048]{1,2,0:T(8,128)(2,1)} async-done(((bf16[2,256,32]{1,2,0:T(8,128)(2,1)}), bf16[2,256,2048]{1,2,0:T(8,128)(2,1)}) %all-gather.5.cloned.1.call-update) | async-done | bytes 2097168 | tf_op jit(solution)/shard_map/all_gather | solution.py:277
  284.2 148.2 %all-gather.7.cloned.1.call-done = bf16[16384,256]{0,1:T(8,128)(2,1)} async-done(((bf16[256,256]{0,1:T(8,128)(2,1)}), bf16[16384,256]{0,1:T(8,128)(2,1)}) %all-gather.7.cloned.1.call-update) | async-done | bytes 8388624 | tf_op jit(solution)/shard_map/all_gather | solution.py:43
  436.9 6.3 copy.178
  447.9 187.3 %while.51 = (s32[]{:T(128)}, f32[1,2,256]{2,1,0:T(2,128)S(1)}, f32[1,2,256]{2,1,0:T(2,128)S(1)}, f32[1,2,256,128]{3,2,1,0:T(8,128)S(1)}, f32[1,2,256]{2,1,0:T(2,...) while((s32[]{:T(128)}, f32[1,2,256]{2,1,0:T(2,128)S(1)}, ...), condition=%wide.region_15.16_spmd.clone, body=%wide.region_8.15_spmd.clone.sunk | while | flops 206442240 | bytes 8724921 | solution.py:232
  448.0 5.8 conditional.3
  453.8 5.8 conditional.3
  459.7 5.8 conditional.3
  465.5 5.8 conditional.3
  471.4 5.8 conditional.3
  477.2 5.8 conditional.3
  483.1 5.8 conditional.3
  488.9 5.8 conditional.3
  494.8 5.8 conditional.3
  500.6 5.8 conditional.3
  506.5 5.8 conditional.3
  512.3 5.8 conditional.3
  518.2 5.8 conditional.3
  524.1 5.8 conditional.3
  529.9 5.8 conditional.3
  535.8 5.8 conditional.3
  541.6 5.8 conditional.3
  547.5 5.8 conditional.3
  553.3 5.8 conditional.3
  559.2 5.8 conditional.3
  565.0 5.8 conditional.3
  570.9 5.8 conditional.3
  576.7 5.8 conditional.3
  637.5 19.5 %all_to_all.5 = bf16[4,64,2048]{2,1,0:T(8,128)(2,1)S(1)} all-to-all(bf16[4,64,2048]{2,1,0:T(8,128)(2,1)S(1)} %bitcast.200), channel_id=1, replica_groups=mesh['grp'=2,'sp'=64,'tp'=4] {'tp'}, dimensions={0} | all-to-all | bytes 2097152 | tf_op jit(solution)/shard_map/all_to_all | solution.py:53
  (775 shorter events, 341.9 us)
Async XLA Ops:
  6.5 4.2 copy-start
  6.5 147.6 %all-gather.9.cloned.1.call-start = ((), (), s32[]{:S(2)}) async-start(), calls=%async_computation.3 | async-start | bytes 4259840 | tf_op jit(solution)/shard_map/all_gather | solution.py:17
  11.3 23.5 %copy-start.1 = (bf16[256,128]{1,0:T(8,128)(2,1)S(1)}, bf16[256,128]{1,0:T(8,128)(2,1)}, u32[]{:S(2)}) copy-start(bf16[256,128]{1,0:T(8,128)(2,1)} %param.32) | copy-start | bytes 196612
  11.3 23.7 %copy-start.4 = (bf16[256,64]{0,1:T(8,128)(2,1)S(1)}, bf16[256,64]{0,1:T(8,128)(2,1)}, u32[]{:S(2)}) copy-start(bf16[256,64]{0,1:T(8,128)(2,1)} %param.31) | copy-start | bytes 98308
  11.3 23.7 %copy-start.5 = (bf16[256,64]{0,1:T(8,128)(2,1)S(1)}, bf16[256,64]{0,1:T(8,128)(2,1)}, u32[]{:S(2)}) copy-start(bf16[256,64]{0,1:T(8,128)(2,1)} %param.29) | copy-start | bytes 98308
  11.3 24.4 %copy-start.2 = (bf16[256,128]{1,0:T(8,128)(2,1)S(1)}, bf16[256,128]{1,0:T(8,128)(2,1)}, u32[]{:S(2)}) copy-start(bf16[256,128]{1,0:T(8,128)(2,1)} %param.28) | copy-start | bytes 196612
  11.3 24.5 %copy-start.3 = (bf16[256,128]{1,0:T(8,128)(2,1)S(1)}, bf16[256,128]{1,0:T(8,128)(2,1)}, u32[]{:S(2)}) copy-start(bf16[256,128]{1,0:T(8,128)(2,1)} %param.30) | copy-start | bytes 196612
  11.3 24.7 %copy-start.6 = (f32[256,2]{0,1:T(2,128)S(1)}, f32[256,2]{0,1:T(2,128)}, u32[]{:S(2)}) copy-start(f32[256,2]{0,1:T(2,128)} %param.26) | copy-start | bytes 6148
  33.9 248.6 %all-gather.5.cloned.1.call-start = ((), (), s32[]{:S(2)}) async-start(), calls=%async_computation.1 | async-start | bytes 2129920 | tf_op jit(solution)/shard_map/all_gather | solution.py:277
  34.7 397.7 %all-gather.7.cloned.1.call-start = ((), (), s32[]{:S(2)}) async-start(), calls=%async_computation.2 | async-start | bytes 8519680 | tf_op jit(solution)/shard_map/all_gather | solution.py:43
  88.6 130.7 %copy-start.7 = (f32[128]{0:T(128)S(1)}, f32[128]{0:T(128)}, u32[]{:S(2)}) copy-start(f32[128]{0:T(128)} %param.27) | copy-start | bytes 1540
  447.9 187.6 %copy-start.9 = (f32[2]{0:T(128)S(1)}, f32[2]{0:T(128)}, u32[]{:S(2)}) copy-start(f32[2]{0:T(128)} %param.33) | copy-start | bytes 28
  447.9 187.7 %copy-start.8 = (f32[128]{0:T(128)S(1)}, f32[128]{0:T(128)}, u32[]{:S(2)}) copy-start(f32[128]{0:T(128)} %param.34) | copy-start | bytes 1540
Sparse Core Ops, SparseCore 0:
  34.0 120.0 all-gather.8
  156.3 126.2 all-gather.4
  284.6 147.8 all-gather.6
where the time goes:
time: 672 us; the launch traced here: 664 us
  waiting for transfers between devices  277 us (41%)
  matrix products  172 us (26%)
  other arithmetic  102 us (15%)
  blocking collectives  71.2 us (11%)
  local copies, waits for them, and re-layouts  20.7 us (3%)
  between operations  13.6 us (2%)
  loops' own time  7.26 us (1%)
    all_gather x1, waiting for transfers between devices, in_one_piece(): lax.all_gather(both, axis, axis=dim, tiled=True)  148 us
    dot_general x64, matrix products, map_update(): jnp.einsum('plew,wpd->pled', weights.astype(jnp.bfloat16), value_rows, pr...  88.7 us
    dot_general x64, matrix products, map_update(): jnp.einsum('qkgd,skd->kgqs', queries, key_rows, preferred_element_type=jn...  75.2 us
    all_gather x1, waiting for transfers between devices, carried_in(): lax.all_gather(part.astype(kind), axis)  64.9 us
    all_gather x1, waiting for transfers between devices, shards(): pieces = lax.all_gather(output_weight, 'sp', axis=2, tiled=True)  63.2 us
    select_n x64, other arithmetic, hop(): return jax.tree.map(lambda a, b: jnp.where(reached, a, b), new, before)  62.1 us
    all_gather x1, blocking collectives, carried_in(): lax.all_gather(part.astype(kind), axis)  51.6 us
    all_to_all x1, blocking collectives, summed_on_arrival(): pieces = lax.all_to_all(split_up(array, dim, size), axis, 0, 0, tiled=True)  19.5 us
  transfers between devices with their start and end apart: 3, of which 3 were waited for; matrix products, arithmetic and copies ran while one was open for 10% of the time, Pallas kernels for 0%

commit v1 on v0

--- a/solution.py
+++ b/solution.py
@@ -274,7 +274,11 @@
         recurrent_added_decay,
         recurrent_norm_gain,
     )
-    pieces = lax.all_gather(output_weight, "sp", axis=2, tiled=True)
+    count = lax.axis_size("sp")
+    repeats = [count if d == 2 else 1 for d in range(output_weight.ndim)]
+    pieces = lax.all_to_all(
+        jnp.tile(output_weight, repeats), "sp", split_axis=2, concat_axis=2, tiled=True
+    )
     partial_terms = jnp.dot(
         recurrent_output, pieces[0], preferred_element_type=jnp.float32
     ) + jnp.dot(attended, pieces[1], preferred_element_type=jnp.float32)

time: 672 us -> 671 us (level)
  waiting for transfers between devices: 277 us -> 43 us
  blocking collectives: 71.2 us -> 264 us
  local copies, waits for them, and re-layouts: 20.7 us -> 51.1 us
  starting transfers between devices: 0.13 us -> 6.92 us
    all_gather x1, blocking collectives: 51.6 us -> 245 us  [carried_in(): lax.all_gather(part.astype(kind), axis)]
    all_gather x1, waiting for transfers between devices: 148 us -> 42.8 us  [in_one_piece(): lax.all_gather(both, axis, axis=dim, tiled=True)]
    all_gather x1, waiting for transfers between devices: 64.9 us -> 0.02 us  [carried_in(): lax.all_gather(part.astype(kind), axis)]
    all_gather x1 -> x0, waiting for transfers between devices: 63.2 us -> none  [shards(): pieces = lax.all_gather(output_weight, 'sp', axis=2, tiled=True)]
    another operation x4 -> x6, local copies, waits for them, and re-layouts: 0.23 us -> 14.5 us  [the longest x2 14.2 us: shards(): jnp.tile(output_weight, repeats)]
    unnamed x26 -> x38, local copies, waits for them, and re-layouts: 8.77 us -> 19.8 us
    all_to_all x0 -> x1, starting transfers between devices: none -> 6.85 us  [shards(): lax.all_to_all(jnp.tile(output_weight, repeats), 'sp', split_axis=2, conc...]
  transfers between devices with their start and end apart: 3 -> 3, of which waited for: 3 -> 1; matrix products, arithmetic and copies ran while one was open for 10% -> 42% of each run, Pallas kernels for 0% -> 0%
where the time goes in v1:
time: 671 us; the launch traced here: 663 us
  blocking collectives  264 us (39%)
  matrix products  174 us (26%)
  other arithmetic  102 us (15%)
  local copies, waits for them, and re-layouts  51.1 us (8%)
  waiting for transfers between devices  43 us (6%)
  between operations  13.9 us (2%)
  loops' own time  7.32 us (1%)
  starting transfers between devices  6.92 us (1%)
    all_gather x1, blocking collectives, carried_in(): lax.all_gather(part.astype(kind), axis)  245 us
    dot_general x64, matrix products, map_update(): jnp.einsum('plew,wpd->pled', weights.astype(jnp.bfloat16), value_rows, pr...  88.7 us
    dot_general x64, matrix products, map_update(): jnp.einsum('qkgd,skd->kgqs', queries, key_rows, preferred_element_type=jn...  75.2 us
    select_n x64, other arithmetic, hop(): return jax.tree.map(lambda a, b: jnp.where(reached, a, b), new, before)  62.1 us
    all_gather x1, waiting for transfers between devices, in_one_piece(): lax.all_gather(both, axis, axis=dim, tiled=True)  42.8 us
    unnamed x38, local copies, waits for them, and re-layouts  19.8 us
    all_to_all x1, blocking collectives, summed_on_arrival(): pieces = lax.all_to_all(split_up(array, dim, size), axis, 0, 0, tiled=True)  19.3 us
    another operation x2, local copies, waits for them, and re-layouts, shards(): jnp.tile(output_weight, repeats)  14.2 us
  transfers between devices with their start and end apart: 3, of which 1 were waited for; matrix products, arithmetic and copies ran while one was open for 42% of the time, Pallas kernels for 0%

profile of v1, /device:TPU:2016, one launch (start us, length us, event | category | flops | bytes accessed | tf_op | source)
XLA Modules:
  0.0 663.5 jit_solution(17784533058292513230)
XLA Ops:
  11.3 26.8 %while.52 = (s32[]{:T(128)}, f32[2,128,128]{2,1,0:T(8,128)S(1)}, f32[8,32,2,128]{3,1,0,2:T(8,128)}, f32[8,32,2,128]{3,2,1,0:T(2,128)S(1)}, f32[8,32,2,128]{3,2,1...) while((s32[]{:T(128)}, f32[2,128,128]{2,1,0:T(8,128)S(1)}, ...), condition=%wide.region_2.3_spmd.clone, body=%wide.region_0.2_spmd.clone.sunk | while | flops 6725635 | bytes 3267192 | solution.py:98
  39.1 14.0 %copy.209 = bf16[2,256,2048]{1,0,2:T(2,128)(2,1)} copy(bf16[2,256,2048]{1,2,0:T(8,128)(2,1)S(1)} %bitcast.201) | data formatting | bytes 4194304 | tf_op jit(solution)/shard_map/tile | solution.py:280
  53.1 6.8 %all-to-all-start = ((bf16[2,256,2048]{1,0,2:T(2,128)(2,1)}), bf16[2,256,2048]{1,0,2:T(2,128)(2,1)S(1)}, u32[]{:S(2)}, u32[]{:S(2)}) async-start(bf16[2,256,2048]{1,0,2:T(2,128)(2,1)} %copy.209), calls=%async_computation | async-start | bytes 4194304 | tf_op jit(solution)/shard_map/all_to_all | solution.py:279
  63.3 245.1 %all_gather.13 = bf16[64,2,128]{2,1,0:T(2,128)(2,1)S(1)} all-gather(bf16[1,2,128]{2,1,0:T(2,128)(2,1)S(1)} %fusion.69), channel_id=1, replica_groups=mesh['grp'=2,'sp'=64,'tp'=4] {'sp'}, dimensions={0}, use_global_device_ids=true | all-gather | bytes 33280 | tf_op jit(solution)/shard_map/all_gather | solution.py:17
  310.0 64.9 %while.53 = (s32[]{:T(128)}, f32[2,128,128]{2,1,0:T(8,128)S(1)}, s32[]{:T(128)}, bf16[64,2,128]{2,1,0:T(2,128)(2,1)S(1)}, bf16[64,2,128,128]{3,2,1,0:T(8,128)(2,1)}, /*index=5*/s32[]{:T(128)}, s32[]{:T(128)}) while((s32[]{:T(128)}, f32[2,128,128]{2,1,0:T(8,128)S(1)}, s32[]{:T(128)}, bf16[64,2,128]{2,1,0:T(2,128)(2,1)S(1)}, ...), condition=%wide.region_6.0_spmd.clone, body=%wide.region_5.6_spmd.clone.sunk | while | flops 164100 | bytes 330345 | solution.py:34
  375.3 42.8 %all-gather.4.cloned.1.call-done = bf16[16384,256]{0,1:T(8,128)(2,1)} async-done(((bf16[256,256]{0,1:T(8,128)(2,1)}), bf16[16384,256]{0,1:T(8,128)(2,1)}) %all-gather.4.cloned.1.call-update) | async-done | bytes 8388624 | tf_op jit(solution)/shard_map/all_gather | solution.py:43
  422.6 6.4 copy.214
  433.7 187.3 %while.51 = (s32[]{:T(128)}, f32[1,2,256]{2,1,0:T(2,128)S(1)}, f32[1,2,256]{2,1,0:T(2,128)S(1)}, f32[1,2,256,128]{3,2,1,0:T(8,128)S(1)}, f32[1,2,256]{2,1,0:T(2,...) while((s32[]{:T(128)}, f32[1,2,256]{2,1,0:T(2,128)S(1)}, ...), condition=%wide.region_15.16_spmd.clone, body=%wide.region_8.15_spmd.clone.sunk | while | flops 206442240 | bytes 8724921 | solution.py:232
  433.7 5.8 conditional.3
  439.6 5.8 conditional.3
  445.4 5.8 conditional.3
  451.3 5.8 conditional.3
  457.2 5.8 conditional.3
  463.0 5.8 conditional.3
  468.9 5.8 conditional.3
  474.7 5.8 conditional.3
  480.6 5.8 conditional.3
  486.4 5.8 conditional.3
  492.3 5.8 conditional.3
  498.1 5.8 conditional.3
  504.0 5.8 conditional.3
  509.8 5.8 conditional.3
  515.7 5.8 conditional.3
  521.5 5.8 conditional.3
  527.4 5.8 conditional.3
  533.2 5.8 conditional.3
  539.1 5.8 conditional.3
  544.9 5.8 conditional.3
  550.8 5.8 conditional.3
  556.6 5.8 conditional.3
  562.5 5.8 conditional.3
  636.4 19.3 %all_to_all.10 = bf16[4,64,2048]{2,1,0:T(8,128)(2,1)S(1)} all-to-all(bf16[4,64,2048]{2,1,0:T(8,128)(2,1)S(1)} %bitcast.202), channel_id=1, replica_groups=mesh['grp'=2,'sp'=64,'tp'=4] {'tp'}, dimensions={0} | all-to-all | bytes 2097152 | tf_op jit(solution)/shard_map/all_to_all | solution.py:53
  (789 shorter events, 359.9 us)
Async XLA Ops:
  6.5 4.2 copy-start.2
  6.5 303.4 %all-gather.6.cloned.1.call-start = ((), (), s32[]{:S(2)}) async-start(), calls=%async_computation.3 | async-start | bytes 4259840 | tf_op jit(solution)/shard_map/all_gather | solution.py:17
  11.3 27.5 %copy-start.8 = (bf16[2,256,32]{1,2,0:T(8,128)(2,1)S(1)}, bf16[2,256,32]{1,2,0:T(8,128)(2,1)}, u32[]{:S(2)}) copy-start(bf16[2,256,32]{1,2,0:T(8,128)(2,1)} %param.35) | copy-start | bytes 98308
  53.1 7.0 %copy-start.3 = (bf16[256,128]{1,0:T(8,128)(2,1)S(1)}, bf16[256,128]{1,0:T(8,128)(2,1)}, u32[]{:S(2)}) copy-start(bf16[256,128]{1,0:T(8,128)(2,1)} %param.32) | copy-start | bytes 196612
  53.1 7.1 %copy-start.9 = (bf16[256,64]{0,1:T(8,128)(2,1)S(1)}, bf16[256,64]{0,1:T(8,128)(2,1)}, u32[]{:S(2)}) copy-start(bf16[256,64]{0,1:T(8,128)(2,1)} %param.31) | copy-start | bytes 98308
  53.1 7.1 %copy-start.10 = (bf16[256,64]{0,1:T(8,128)(2,1)S(1)}, bf16[256,64]{0,1:T(8,128)(2,1)}, u32[]{:S(2)}) copy-start(bf16[256,64]{0,1:T(8,128)(2,1)} %param.29) | copy-start | bytes 98308
  53.1 7.9 %copy-start.4 = (bf16[256,128]{1,0:T(8,128)(2,1)S(1)}, bf16[256,128]{1,0:T(8,128)(2,1)}, u32[]{:S(2)}) copy-start(bf16[256,128]{1,0:T(8,128)(2,1)} %param.28) | copy-start | bytes 196612
  53.1 8.6 %copy-start.5 = (bf16[256,128]{1,0:T(8,128)(2,1)S(1)}, bf16[256,128]{1,0:T(8,128)(2,1)}, u32[]{:S(2)}) copy-start(bf16[256,128]{1,0:T(8,128)(2,1)} %param.30) | copy-start | bytes 196612
  53.1 9.3 %copy-start.11 = (f32[256,2]{0,1:T(2,128)S(1)}, f32[256,2]{0,1:T(2,128)}, u32[]{:S(2)}) copy-start(f32[256,2]{0,1:T(2,128)} %param.26) | copy-start | bytes 6148
  53.1 568.3 %all-to-all-start = ((bf16[2,256,2048]{1,0,2:T(2,128)(2,1)}), bf16[2,256,2048]{1,0,2:T(2,128)(2,1)S(1)}, u32[]{:S(2)}, u32[]{:S(2)}) async-start(bf16[2,256,2048]{1,0,2:T(2,128)(2,1)} %copy.209), calls=%async_computation | async-start | bytes 4194304 | tf_op jit(solution)/shard_map/all_to_all | solution.py:279
  60.0 358.2 %all-gather.4.cloned.1.call-start = ((), (), s32[]{:S(2)}) async-start(), calls=%async_computation.2 | async-start | bytes 8519680 | tf_op jit(solution)/shard_map/all_gather | solution.py:43
  308.4 66.8 %copy-start.12 = (f32[128]{0:T(128)S(1)}, f32[128]{0:T(128)}, u32[]{:S(2)}) copy-start(f32[128]{0:T(128)} %param.27) | copy-start | bytes 1540
  429.0 4.7 copy-start.6
  429.0 4.7 copy-start.7
  433.7 187.6 %copy-start.14 = (f32[2]{0:T(128)S(1)}, f32[2]{0:T(128)}, u32[]{:S(2)}) copy-start(f32[2]{0:T(128)} %param.33) | copy-start | bytes 28
  625.6 4.7 copy-start
  634.7 0.7 copy-start.13
  634.7 1.2 copy-start.1
Sparse Core Ops, SparseCore 0:
  38.9 218.6 all-gather.5
  259.6 158.4 all-gather.3
